TPU v7x, 32 devices: a whole 2x2x4 slice. The times are simulated.
32 devices in a mesh: fs: 16 (over z, y, x), tp: 2 (over core).
Axes of the slice: x: 2, y: 2, z: 4, core: 2. Of those that a mesh axis runs over, the one named last changes fastest.
Arguments:
- tokens: bfloat16 [2048, 2048], P('fs'), may hold values from -6 to 6
- norm_gain: float32 [2048], replicated, may hold values from 0.1 to 1.9
- w_query: bfloat16 [2048, 1024], P('fs', 'tp'), may hold values from -0.125 to 0.125
- w_key: bfloat16 [2048, 1024], P('fs', 'tp'), may hold values from -0.125 to 0.125
- w_value: bfloat16 [2048, 2048], P('fs', 'tp'), may hold values from -0.125 to 0.125
- w_gate: bfloat16 [2048, 2048], P('fs', 'tp'), may hold values from -0.125 to 0.125
- mixer_gain: float32 [2048], P('tp'), may hold values from 0.1 to 1.9
- w_out: bfloat16 [2048, 2048], P('tp', 'fs'), may hold values from -0.125 to 0.125
- channel_gain: float32 [2048], replicated, may hold values from 0.1 to 1.9
- w_left: bfloat16 [2048, 3072], P('fs', 'tp'), may hold values from -0.125 to 0.125
- w_right: bfloat16 [2048, 3072], P('fs', 'tp'), may hold values from -0.125 to 0.125
- taps_left: float32 [3, 3072], P(None, 'tp'), may hold values from -3.5 to 3.5
- taps_right: float32 [3, 3072], P(None, 'tp'), may hold values from -3.5 to 3.5
- w_down: bfloat16 [3072, 2048], P('tp', 'fs'), may hold values from -0.109375 to 0.109375
Outputs:
- layer_out: bfloat16 [2048, 2048], P('fs')
All inputs are finite; a program needn't handle non-finite values.
Results may differ from a plain program's by a relative error of at most 0.018.
Values may be sent and summed in bfloat16 or wider, within the bound.
A program may use at most 64 MiB of HBM per device.

v0:
```python
import jax
import jax.numpy as jnp
from jax import lax
from jax.sharding import PartitionSpec as P

DK = 128
DV = 256
BLOCK = 128
highest = lax.Precision.HIGHEST


def scale_rows(rows_in, gain_vec):
    floats = rows_in.astype(jnp.float32)
    factor = lax.rsqrt(jnp.mean(floats * floats, axis=-1, keepdims=True) + 1e-06)
    return (floats * factor * gain_vec).astype(jnp.bfloat16)


def decays(first_head, count):
    head_ids = first_head + jnp.arange(count, dtype=jnp.float32)
    return jnp.log(1.0 - 2.0 ** (-5.0 - head_ids))


def rotate(heads_in, positions):
    width = heads_in.shape[-1]
    half = width // 2
    freqs = 10000.0 ** (-jnp.arange(half, dtype=jnp.float32) / half)
    angles = positions[:, None] * freqs[None, :]
    cosine = jnp.cos(angles)
    sine = jnp.sin(angles)
    first_half = heads_in[..., :half]
    second_half = heads_in[..., half:]
    return jnp.concatenate(
        [first_half * cosine - second_half * sine, first_half * sine + second_half * cosine],
        axis=-1,
    )


def retention(queries, keys_in, values_in, log_gamma):
    head_count, length, key_width = queries.shape
    value_width = values_in.shape[-1]
    blocks = length // BLOCK
    queries = queries.reshape(head_count, blocks, BLOCK, key_width)
    keys_in = keys_in.reshape(head_count, blocks, BLOCK, key_width)
    values_in = values_in.reshape(head_count, blocks, BLOCK, value_width)
    offsets = jnp.arange(BLOCK, dtype=jnp.float32)
    distance = offsets[:, None] - offsets[None, :]
    weights = jnp.where(
        distance >= 0, jnp.exp(log_gamma[:, None, None] * jnp.maximum(distance, 0.0)), 0.0
    )
    scores = jnp.einsum("hbnd,hbmd->hbnm", queries, keys_in, precision=highest) * weights[:, None]
    inner = jnp.einsum("hbnm,hbme->hbne", scores, values_in, precision=highest)
    key_weight = jnp.exp(log_gamma[:, None] * (BLOCK - 1 - offsets)[None, :])
    contrib = jnp.einsum(
        "hbjd,hbje->hbde", keys_in * key_weight[:, None, :, None], values_in, precision=highest
    )
    block_decay = jnp.exp(log_gamma * BLOCK)[:, None, None]

    def advance(state, contrib_block):
        return (state * block_decay + contrib_block, state)

    _, states = lax.scan(
        advance,
        jnp.zeros((head_count, key_width, value_width), jnp.float32),
        jnp.moveaxis(contrib, 1, 0),
    )
    states = jnp.moveaxis(states, 0, 1)
    query_weight = jnp.exp(log_gamma[:, None] * (offsets + 1.0)[None, :])
    carried = (
        jnp.einsum("hbnd,hbde->hbne", queries, states, precision=highest)
        * query_weight[:, None, :, None]
    )
    return (inner + carried).reshape(head_count, length, value_width)


def head_norm(retained):
    return retained * lax.rsqrt(jnp.mean(retained * retained, axis=-1, keepdims=True) + 1e-06)


def causal_taps(values_in, taps):
    length = values_in.shape[-2]
    padded = jnp.pad(values_in.astype(jnp.float32), ((taps.shape[0] - 1, 0), (0, 0)))
    result = padded[0:length] * taps[0]
    for tap_index in range(1, taps.shape[0]):
        result = result + padded[tap_index : tap_index + length] * taps[tap_index]
    return result


def fold_single(source, weight_piece):
    return jnp.dot(source, weight_piece, preferred_element_type=jnp.float32)


def collect_single(source, weight):
    return fold_single(source, lax.all_gather(weight, "fs", axis=0, tiled=True))


def body(
    tokens,
    norm_gain,
    w_query,
    w_key,
    w_value,
    w_gate,
    mixer_gain,
    w_out,
    channel_gain,
    w_left,
    w_right,
    taps_left,
    taps_right,
    w_down,
):
    length = tokens.shape[0]
    normed = scale_rows(tokens, norm_gain)
    queries = collect_single(normed, w_query)
    keys_proj = collect_single(normed, w_key)
    values_proj = collect_single(normed, w_value)
    gates = collect_single(normed, w_gate)
    queries = queries.astype(jnp.bfloat16)
    keys_proj = keys_proj.astype(jnp.bfloat16)
    values_proj = values_proj.astype(jnp.bfloat16)
    gates = gates.astype(jnp.bfloat16)
    heads_here = w_query.shape[1] // DK
    first_head = (lax.axis_index("tp") * heads_here).astype(jnp.float32)
    log_gamma = decays(first_head, heads_here)
    positions = jnp.arange(length, dtype=jnp.float32)

    def split_heads(rows_in, width):
        return rows_in.astype(jnp.float32).reshape(length, heads_here, width).transpose(1, 0, 2)

    retained = head_norm(
        retention(
            rotate(split_heads(queries, DK), positions),
            rotate(split_heads(keys_proj, DK), positions),
            split_heads(values_proj, DV),
            log_gamma,
        )
    )
    retained = retained.transpose(1, 0, 2).reshape(length, heads_here * DV)
    hidden = (retained * mixer_gain * jax.nn.silu(gates.astype(jnp.float32))).astype(jnp.bfloat16)
    rows_own = length // lax.axis_size("tp")
    first_row = lax.axis_index("tp") * rows_own
    out_whole = lax.all_gather(w_out, "fs", axis=1, tiled=True)
    mixer_total = lax.psum_scatter(
        jnp.dot(hidden, out_whole, preferred_element_type=jnp.float32).astype(jnp.bfloat16),
        "tp",
        scatter_dimension=0,
        tiled=True,
    ).astype(jnp.float32)
    residual = lax.dynamic_slice_in_dim(tokens, first_row, rows_own, 0)
    middle_own = (residual.astype(jnp.float32) + mixer_total).astype(jnp.bfloat16)
    middle = lax.all_gather(middle_own, "tp", axis=0, tiled=True)
    normed_mid = scale_rows(middle, channel_gain)
    left = collect_single(normed_mid, w_left)
    right = collect_single(normed_mid, w_right)
    left = left.astype(jnp.bfloat16)
    right = right.astype(jnp.bfloat16)
    gated = (jax.nn.silu(causal_taps(left, taps_left)) * causal_taps(right, taps_right)).astype(
        jnp.bfloat16
    )
    down_whole = lax.all_gather(w_down, "fs", axis=1, tiled=True)
    channel_part = jnp.dot(gated, down_whole, preferred_element_type=jnp.float32)
    channel_total = lax.psum(channel_part.astype(jnp.bfloat16), "tp").astype(jnp.float32)
    return (middle.astype(jnp.float32) + channel_total).astype(jnp.bfloat16)


def solution(mesh):
    placed = (
        P("fs", None),
        P(),
        P("fs", "tp"),
        P("fs", "tp"),
        P("fs", "tp"),
        P("fs", "tp"),
        P("tp"),
        P("tp", "fs"),
        P(),
        P("fs", "tp"),
        P("fs", "tp"),
        P(None, "tp"),
        P(None, "tp"),
        P("tp", "fs"),
    )
    return jax.shard_map(body, mesh=mesh, in_specs=placed, out_specs=P("fs", None), check_vma=False)
```

profile of v0, /device:TPU:0, one launch (start us, length us, event | category | flops | bytes accessed | tf_op | source)
XLA Modules:
  0.0 730.4 jit_solution(5038678450189377104)
XLA Ops:
  6.5 0.7 all-gather.11.cloned.1.call-update
  7.3 0.0 all-gather.9.cloned.1.call-start
  7.3 0.7 all-gather.9.cloned.1.call-update
  8.0 0.0 all-gather.13.cloned.1.call-start
  8.1 0.7 all-gather.13.cloned.1.call-update
  8.8 0.5 all-gather.15.cloned.1.call-update
  9.3 0.0 all-gather.17.cloned.1.call-start
  9.4 0.5 all-gather.17.cloned.1.call-update
  9.9 0.0 reduce-scatter.2.cloned.1.call-start
  10.1 1.2 fusion.7
  11.3 0.1 multiply_exponential_fusion
  11.4 0.1 multiply_exponential_fusion.1
  11.5 0.3 fusion.49
  11.7 61.5 %all-gather.11.cloned.1.call-done = bf16[2048,512]{1,0:T(8,128)(2,1)} async-done(((bf16[128,512]{1,0:T(8,128)(2,1)}), bf16[2048,512]{1,0:T(8,128)(2,1)}) %all-gather.11.cloned.1.call-update) | async-done | bytes 2097168 | tf_op jit(solution)/shard_map/all_gather | solution.py:93
  73.2 2.3 fusion.4
  75.5 59.7 %all-gather.9.cloned.1.call-done = bf16[2048,512]{1,0:T(8,128)(2,1)} async-done(((bf16[128,512]{1,0:T(8,128)(2,1)}), bf16[2048,512]{1,0:T(8,128)(2,1)}) %all-gather.9.cloned.1.call-update) | async-done | bytes 2097168 | tf_op jit(solution)/shard_map/all_gather | solution.py:93
  135.2 2.1 fusion.6
  137.3 0.3 multiply_subtract_fusion
  137.6 0.4 fusion.42
  138.1 0.7 convolution_multiply_fusion
  138.8 73.6 %all-gather.13.cloned.1.call-done = bf16[2048,1024]{1,0:T(8,128)(2,1)} async-done(((bf16[128,1024]{1,0:T(8,128)(2,1)}), bf16[2048,1024]{1,0:T(8,128)(2,1)}) %all-gather.13.cloned.1.call-update) | async-done | bytes 4194320 | tf_op jit(solution)/shard_map/all_gather | solution.py:93
  212.4 2.9 convolution_convert_fusion.5
  215.4 0.5 multiply_reduce_fusion
  215.8 0.2 fusion.25
  216.1 0.2 copy.21
  216.3 0.2 copy.22
  216.5 72.8 %all-gather.15.cloned.1.call-done = bf16[2048,1024]{1,0:T(8,128)(2,1)} async-done(((bf16[128,1024]{1,0:T(8,128)(2,1)}), bf16[2048,1024]{1,0:T(8,128)(2,1)}) %all-gather.15.cloned.1.call-update) | async-done | bytes 4194320 | tf_op jit(solution)/shard_map/all_gather | solution.py:93
  289.3 89.9 %all-gather.17.cloned.1.call-done = bf16[1024,2048]{1,0:T(8,128)(2,1)} async-done(((bf16[1024,128]{1,0:T(8,128)(2,1)}), bf16[1024,2048]{1,0:T(8,128)(2,1)}) %all-gather.17.cloned.1.call-update) | async-done | bytes 4194320 | tf_op jit(solution)/shard_map/all_gather | solution.py:142
  379.2 5.7 convolution_convert_fusion.1
  384.9 0.0 all-gather.19.cloned.1.call-start
  384.9 0.7 all-gather.19.cloned.1.call-update
  385.6 0.0 all-gather.21.cloned.1.call-start
  385.7 0.7 all-gather.21.cloned.1.call-update
  386.4 0.7 all-gather.23.cloned.1.call-update
  387.1 0.0 all-reduce.4.cloned.1.call-start
  387.2 0.1 slice_reduce_fusion.2
  387.3 3.9 reduce-scatter.2.cloned.1.call-done
  391.2 1.0 add_convert_fusion
  392.2 2.2 all_gather.32
  394.4 0.2 fusion.10
  394.5 93.9 %all-gather.19.cloned.1.call-done = bf16[2048,1536]{1,0:T(8,128)(2,1)} async-done(((bf16[128,1536]{1,0:T(8,128)(2,1)}), bf16[2048,1536]{1,0:T(8,128)(2,1)}) %all-gather.19.cloned.1.call-update) | async-done | bytes 6291472 | tf_op jit(solution)/shard_map/all_gather | solution.py:93
  488.5 3.8 fusion.1
  492.3 90.9 %all-gather.21.cloned.1.call-done = bf16[2048,1536]{1,0:T(8,128)(2,1)} async-done(((bf16[128,1536]{1,0:T(8,128)(2,1)}), bf16[2048,1536]{1,0:T(8,128)(2,1)}) %all-gather.21.cloned.1.call-update) | async-done | bytes 6291472 | tf_op jit(solution)/shard_map/all_gather | solution.py:93
  583.2 3.8 fusion
  587.0 112.5 %all-gather.23.cloned.1.call-done = bf16[1536,2048]{1,0:T(8,128)(2,1)} async-done(((bf16[1536,128]{1,0:T(8,128)(2,1)}), bf16[1536,2048]{1,0:T(8,128)(2,1)}) %all-gather.23.cloned.1.call-update) | async-done | bytes 6291472 | tf_op jit(solution)/shard_map/all_gather | solution.py:160
  699.5 5.1 convolution_convert_fusion
  704.6 16.9 %all-reduce.4.cloned.1.call-done = bf16[128,2048]{1,0:T(8,128)(2,1)} async-done(((bf16[128,2048]{1,0:T(8,128)(2,1)}), bf16[128,2048]{1,0:T(8,128)(2,1)}) %all-reduce.4.cloned.1.call-update) | async-done | bytes 524304 | tf_op jit(solution)/shard_map/psum | solution.py:162
  721.6 2.0 fusion.13
  (27 shorter events, 0.3 us)
Async XLA Ops:
  6.5 128.7 %copy-start = (bf16[128,2048]{1,0:T(8,128)(2,1)S(1)}, bf16[128,2048]{1,0:T(8,128)(2,1)}, u32[]{:S(2)}) copy-start(bf16[128,2048]{1,0:T(8,128)(2,1)} %param.14) | copy-start | bytes 1572868
  6.5 128.7 %copy-start.1 = (f32[2048]{0:T(1024)S(1)}, f32[2048]{0:T(1024)}, u32[]{:S(2)}) copy-start(f32[2048]{0:T(1024)} %param.15) | copy-start | bytes 24580
  6.5 66.7 %all-gather.11.cloned.1.call-start = ((), (), s32[]{:S(2)}) async-start(), calls=%async_computation.2 | async-start | bytes 2228224 | tf_op jit(solution)/shard_map/all_gather | solution.py:93
  7.3 128.0 %all-gather.9.cloned.1.call-start = ((), (), s32[]{:S(2)}) async-start(), calls=%async_computation.1 | async-start | bytes 2228224 | tf_op jit(solution)/shard_map/all_gather | solution.py:93
  8.0 204.4 %all-gather.13.cloned.1.call-start = ((), (), s32[]{:S(2)}) async-start(), calls=%async_computation.3 | async-start | bytes 4456448 | tf_op jit(solution)/shard_map/all_gather | solution.py:93
  8.7 280.5 %all-gather.15.cloned.1.call-start = ((), (), s32[]{:S(2)}) async-start(), calls=%async_computation.4 | async-start | bytes 4456448 | tf_op jit(solution)/shard_map/all_gather | solution.py:93
  9.3 369.8 %all-gather.17.cloned.1.call-start = ((), (), s32[]{:S(2)}) async-start(), calls=%async_computation.5 | async-start | bytes 4456448 | tf_op jit(solution)/shard_map/all_gather | solution.py:142
  9.9 381.2 %reduce-scatter.2.cloned.1.call-start = ((), (), s32[]{:S(2)}) async-start(), calls=%async_computation.6 | async-start | bytes 786432 | tf_op jit(solution)/shard_map/reduce_scatter | solution.py:143
  138.8 240.4 %copy-start.5 = (f32[1024]{0:T(1024)S(1)}, f32[1024]{0:T(1024)}, u32[]{:S(2)}) copy-start(f32[1024]{0:T(1024)} %param.20) | copy-start | bytes 12292
  216.5 170.7 %copy-start.3 = (f32[3,1536]{1,0:T(4,128)S(1)}, f32[3,1536]{1,0:T(4,128)}, u32[]{:S(2)}) copy-start(f32[3,1536]{1,0:T(4,128)} %param.26) | copy-start | bytes 55300
  216.5 170.7 %copy-start.4 = (f32[3,1536]{1,0:T(4,128)S(1)}, f32[3,1536]{1,0:T(4,128)}, u32[]{:S(2)}) copy-start(f32[3,1536]{1,0:T(4,128)} %param.25) | copy-start | bytes 55300
  216.5 272.0 %copy-start.2 = (f32[2048]{0:T(1024)S(1)}, f32[2048]{0:T(1024)}, u32[]{:S(2)}) copy-start(f32[2048]{0:T(1024)} %param.22) | copy-start | bytes 24580
  384.9 103.6 %all-gather.19.cloned.1.call-start = ((), (), s32[]{:S(2)}) async-start(), calls=%async_computation.7 | async-start | bytes 6684672 | tf_op jit(solution)/shard_map/all_gather | solution.py:93
  385.6 197.6 %all-gather.21.cloned.1.call-start = ((), (), s32[]{:S(2)}) async-start(), calls=%async_computation.8 | async-start | bytes 6684672 | tf_op jit(solution)/shard_map/all_gather | solution.py:93
  386.4 313.1 %all-gather.23.cloned.1.call-start = ((), (), s32[]{:S(2)}) async-start(), calls=%async_computation.9 | async-start | bytes 6684672 | tf_op jit(solution)/shard_map/all_gather | solution.py:160
  387.1 334.4 %all-reduce.4.cloned.1.call-start = ((), (), s32[]{:S(2)}) async-start(), calls=%async_computation.10 | async-start | bytes 1048576 | tf_op jit(solution)/shard_map/psum | solution.py:162
Sparse Core Ops, SparseCore 0:
  10.1 63.0 all-gather.10
  76.0 59.1 all-gather.8
  138.0 74.3 all-gather.12
  215.0 74.1 all-gather.14
  291.8 87.3 all-gather.16
  385.0 6.0 reduce-scatter.1
  393.9 94.5 all-gather.18
  491.3 91.9 all-gather.20
  585.9 113.5 all-gather.22
  704.8 16.7 all-reduce.3
where the time goes:
time: 731 us; the launch traced here: 730 us
  waiting for transfers between devices  681 us (93%)
  matrix products  27.3 us (4%)
  between operations  13.7 us (2%)
    all_gather x6, waiting for transfers between devices, collect_single(): return fold_single(source, lax.all_gather(weight, 'fs', axis=0, tiled=True))  452 us
    all_gather x1, waiting for transfers between devices, body(): down_whole = lax.all_gather(w_down, 'fs', axis=1, tiled=True)  112 us
    all_gather x1, waiting for transfers between devices, body(): out_whole = lax.all_gather(w_out, 'fs', axis=1, tiled=True)  89.9 us
    psum x1, waiting for transfers between devices, body(): lax.psum(channel_part.astype(jnp.bfloat16), 'tp').astype(jnp.float32)  16.9 us
    dot_general x5, matrix products, fold_single(): return jnp.dot(source, weight_piece, preferred_element_type=jnp.float32)  14.9 us
  transfers between devices with their start and end apart: 10, of which 10 were waited for; matrix products, arithmetic and copies ran while one was open for 3% of the time, Pallas kernels for 0%

commit v1 on v0

--- a/solution.py
+++ b/solution.py
@@ -139,7 +139,13 @@
     hidden = (retained * mixer_gain * jax.nn.silu(gates.astype(jnp.float32))).astype(jnp.bfloat16)
     rows_own = length // lax.axis_size("tp")
     first_row = lax.axis_index("tp") * rows_own
-    out_whole = lax.all_gather(w_out, "fs", axis=1, tiled=True)
+    size = lax.axis_size("fs")
+    current, pieces = (w_out, [w_out])
+    for _ in range(size - 1):
+        current = lax.ppermute(current, "fs", [(i, (i + 1) % size) for i in range(size)])
+        pieces.insert(0, current)
+    merged = jnp.concatenate(pieces, axis=1)
+    out_whole = jnp.roll(merged, (lax.axis_index("fs") + 1) * w_out.shape[1], axis=1)
     mixer_total = lax.psum_scatter(
         jnp.dot(hidden, out_whole, preferred_element_type=jnp.float32).astype(jnp.bfloat16),
         "tp",

time: 731 us -> 663 us (0.907)
  waiting for transfers between devices: 681 us -> 575 us
  local copies, waits for them, and re-layouts: 0.56 us -> 32.4 us
    all_gather x6, waiting for transfers between devices: 452 us -> 247 us  [collect_single(): return fold_single(source, lax.all_gather(weight, 'fs', axis=0, tiled=True))]
    ppermute x0 -> x15, waiting for transfers between devices: none -> 190 us  [body(): lax.ppermute(current, 'fs', [(i, (i + 1) % size) for i in range(size)])]
    all_gather x1 -> x0, waiting for transfers between devices: 89.9 us -> none  [body(): out_whole = lax.all_gather(w_out, 'fs', axis=1, tiled=True)]
    unnamed x12 -> x61, local copies, waits for them, and re-layouts: 0.03 us -> 31.1 us
  transfers between devices with their start and end apart: 10 -> 24, of which waited for: 10 -> 21; matrix products, arithmetic and copies ran while one was open for 3% -> 8% of each run, Pallas kernels for 0% -> 0%
where the time goes in v1:
time: 663 us; the launch traced here: 662 us
  waiting for transfers between devices  575 us (87%)
  local copies, waits for them, and re-layouts  32.4 us (5%)
  matrix products  27.9 us (4%)
  between operations  13.5 us (2%)
  other arithmetic  7.94 us (1%)
    all_gather x6, waiting for transfers between devices, collect_single(): return fold_single(source, lax.all_gather(weight, 'fs', axis=0, tiled=True))  247 us
    ppermute x15, waiting for transfers between devices, body(): lax.ppermute(current, 'fs', [(i, (i + 1) % size) for i in range(size)])  190 us
    all_gather x1, waiting for transfers between devices, body(): down_whole = lax.all_gather(w_down, 'fs', axis=1, tiled=True)  112 us
    unnamed x61, local copies, waits for them, and re-layouts  31.1 us
    psum x1, waiting for transfers between devices, body(): lax.psum(channel_part.astype(jnp.bfloat16), 'tp').astype(jnp.float32)  16.9 us
    dot_general x5, matrix products, fold_single(): return jnp.dot(source, weight_piece, preferred_element_type=jnp.float32)  14.8 us
  transfers between devices with their start and end apart: 24, of which 21 were waited for; matrix products, arithmetic and copies ran while one was open for 8% of the time, Pallas kernels for 0%

profile of v1, /device:TPU:0, one launch (start us, length us, event | category | flops | bytes accessed | tf_op | source)
XLA Modules:
  0.0 662.4 jit_solution(38680455617118590)
XLA Ops:
  8.8 3.0 collective-permute-start
  11.8 10.5 %collective-permute-done = bf16[1024,128]{1,0:T(8,128)(2,1)S(1)} collective-permute-done((bf16[1024,128]{1,0:T(8,128)(2,1)}, bf16[1024,128]{1,0:T(8,128)(2,1)S(1)}, u32[]{:S(2)}, u32[]{:S(2)}) %collective-permute-start) | collective-permute-done | bytes 262176 | tf_op jit(solution)/shard_map/ppermute | solution.py:145
  22.3 13.8 %collective-permute-done.1 = bf16[1024,128]{1,0:T(8,128)(2,1)S(1)} collective-permute-done((bf16[1024,128]{1,0:T(8,128)(2,1)S(1)}, bf16[1024,128]{1,0:T(8,128)(2,1)S(1)}, u32[]{:S(2)}, u32[]{:S(2)}) %collective-permute-start.1) | collective-permute-done | bytes 262176 | tf_op jit(solution)/shard_map/ppermute | solution.py:145
  36.2 14.3 %collective-permute-done.2 = bf16[1024,128]{1,0:T(8,128)(2,1)S(1)} collective-permute-done((bf16[1024,128]{1,0:T(8,128)(2,1)S(1)}, bf16[1024,128]{1,0:T(8,128)(2,1)S(1)}, u32[]{:S(2)}, u32[]{:S(2)}) %collective-permute-start.2) | collective-permute-done | bytes 262176 | tf_op jit(solution)/shard_map/ppermute | solution.py:145
  50.4 10.0 %collective-permute-done.3 = bf16[1024,128]{1,0:T(8,128)(2,1)S(1)} collective-permute-done((bf16[1024,128]{1,0:T(8,128)(2,1)S(1)}, bf16[1024,128]{1,0:T(8,128)(2,1)S(1)}, u32[]{:S(2)}, u32[]{:S(2)}) %collective-permute-start.3) | collective-permute-done | bytes 262176 | tf_op jit(solution)/shard_map/ppermute | solution.py:145
  60.4 16.8 %collective-permute-done.4 = bf16[1024,128]{1,0:T(8,128)(2,1)S(1)} collective-permute-done((bf16[1024,128]{1,0:T(8,128)(2,1)S(1)}, bf16[1024,128]{1,0:T(8,128)(2,1)S(1)}, u32[]{:S(2)}, u32[]{:S(2)}) %collective-permute-start.4) | collective-permute-done | bytes 262176 | tf_op jit(solution)/shard_map/ppermute | solution.py:145
  77.2 11.5 %collective-permute-done.5 = bf16[1024,128]{1,0:T(8,128)(2,1)S(1)} collective-permute-done((bf16[1024,128]{1,0:T(8,128)(2,1)S(1)}, bf16[1024,128]{1,0:T(8,128)(2,1)S(1)}, u32[]{:S(2)}, u32[]{:S(2)}) %collective-permute-start.5) | collective-permute-done | bytes 262176 | tf_op jit(solution)/shard_map/ppermute | solution.py:145
  88.7 14.5 %collective-permute-done.6 = bf16[1024,128]{1,0:T(8,128)(2,1)S(1)} collective-permute-done((bf16[1024,128]{1,0:T(8,128)(2,1)S(1)}, bf16[1024,128]{1,0:T(8,128)(2,1)S(1)}, u32[]{:S(2)}, u32[]{:S(2)}) %collective-permute-start.6) | collective-permute-done | bytes 262176 | tf_op jit(solution)/shard_map/ppermute | solution.py:145
  103.2 12.0 %collective-permute-done.7 = bf16[1024,128]{1,0:T(8,128)(2,1)S(1)} collective-permute-done((bf16[1024,128]{1,0:T(8,128)(2,1)S(1)}, bf16[1024,128]{1,0:T(8,128)(2,1)S(1)}, u32[]{:S(2)}, u32[]{:S(2)}) %collective-permute-start.7) | collective-permute-done | bytes 262176 | tf_op jit(solution)/shard_map/ppermute | solution.py:145
  115.2 13.7 %collective-permute-done.8 = bf16[1024,128]{1,0:T(8,128)(2,1)S(1)} collective-permute-done((bf16[1024,128]{1,0:T(8,128)(2,1)S(1)}, bf16[1024,128]{1,0:T(8,128)(2,1)S(1)}, u32[]{:S(2)}, u32[]{:S(2)}) %collective-permute-start.8) | collective-permute-done | bytes 262176 | tf_op jit(solution)/shard_map/ppermute | solution.py:145
  129.1 15.7 %collective-permute-done.9 = bf16[1024,128]{1,0:T(8,128)(2,1)S(1)} collective-permute-done((bf16[1024,128]{1,0:T(8,128)(2,1)S(1)}, bf16[1024,128]{1,0:T(8,128)(2,1)S(1)}, u32[]{:S(2)}, u32[]{:S(2)}) %collective-permute-start.9) | collective-permute-done | bytes 262176 | tf_op jit(solution)/shard_map/ppermute | solution.py:145
  144.8 1.2 fusion.12
  146.0 9.9 %collective-permute-done.10 = bf16[1024,128]{1,0:T(8,128)(2,1)S(1)} collective-permute-done((bf16[1024,128]{1,0:T(8,128)(2,1)S(1)}, bf16[1024,128]{1,0:T(8,128)(2,1)S(1)}, u32[]{:S(2)}, u32[]{:S(2)}) %collective-permute-start.10) | collective-permute-done | bytes 262176 | tf_op jit(solution)/shard_map/ppermute | solution.py:145
  156.5 9.4 %collective-permute-done.11 = bf16[1024,128]{1,0:T(8,128)(2,1)S(1)} collective-permute-done((bf16[1024,128]{1,0:T(8,128)(2,1)S(1)}, bf16[1024,128]{1,0:T(8,128)(2,1)S(1)}, u32[]{:S(2)}, u32[]{:S(2)}) %collective-permute-start.11) | collective-permute-done | bytes 262176 | tf_op jit(solution)/shard_map/ppermute | solution.py:145
  166.0 14.7 %collective-permute-done.12 = bf16[1024,128]{1,0:T(8,128)(2,1)S(1)} collective-permute-done((bf16[1024,128]{1,0:T(8,128)(2,1)S(1)}, bf16[1024,128]{1,0:T(8,128)(2,1)S(1)}, u32[]{:S(2)}, u32[]{:S(2)}) %collective-permute-start.12) | collective-permute-done | bytes 262176 | tf_op jit(solution)/shard_map/ppermute | solution.py:145
  182.1 13.5 %collective-permute-done.13 = bf16[1024,128]{1,0:T(8,128)(2,1)} collective-permute-done((bf16[1024,128]{1,0:T(8,128)(2,1)S(1)}, bf16[1024,128]{1,0:T(8,128)(2,1)}, u32[]{:S(2)}, u32[]{:S(2)}) %collective-permute-start.13) | collective-permute-done | bytes 262176 | tf_op jit(solution)/shard_map/ppermute | solution.py:145
  195.7 0.9 fusion.54
  196.5 9.3 %collective-permute-done.14 = bf16[1024,128]{1,0:T(8,128)(2,1)} collective-permute-done((bf16[1024,128]{1,0:T(8,128)(2,1)}, bf16[1024,128]{1,0:T(8,128)(2,1)}, u32[]{:S(2)}, u32[]{:S(2)}) %collective-permute-start.14) | collective-permute-done | bytes 262176 | tf_op jit(solution)/shard_map/ppermute | solution.py:145
  205.9 1.8 constant_dynamic-update-slice_fusion.31
  207.7 1.7 constant_dynamic-update-slice_fusion.30
  209.4 1.7 constant_dynamic-update-slice_fusion.29
  211.1 1.7 constant_dynamic-update-slice_fusion.28
  212.8 1.7 constant_dynamic-update-slice_fusion.27
  217.6 0.8 constant_dynamic-update-slice_fusion.22
  221.3 0.8 constant_dynamic-update-slice_fusion.17
  222.9 1.7 constant_dynamic-update-slice_fusion.15
  224.6 1.7 constant_dynamic-update-slice_fusion.14
  226.3 0.8 constant_dynamic-update-slice_fusion.13
  227.8 0.8 constant_dynamic-update-slice_fusion.11
  228.6 0.8 constant_dynamic-update-slice_fusion.10
  237.0 2.1 fusion.9
  239.1 2.1 fusion.11
  241.3 1.1 multiply_subtract_fusion
  242.8 1.5 convolution_multiply_fusion
  244.3 3.0 convolution_convert_fusion.4
  248.4 62.8 %all-gather.14.cloned.1.call-done = bf16[2048,1024]{1,0:T(8,128)(2,1)} async-done(((bf16[128,1024]{1,0:T(8,128)(2,1)}), bf16[2048,1024]{1,0:T(8,128)(2,1)}) %all-gather.14.cloned.1.call-update) | async-done | bytes 4194320 | tf_op jit(solution)/shard_map/all_gather | solution.py:93
  311.3 5.7 fusion.2
  319.2 4.4 reduce-scatter.2.cloned.1.call-done
  323.7 1.0 add_convert_fusion
  324.7 2.4 all_gather.28
  327.2 93.6 %all-gather.16.cloned.1.call-done = bf16[2048,1536]{1,0:T(8,128)(2,1)} async-done(((bf16[128,1536]{1,0:T(8,128)(2,1)}), bf16[2048,1536]{1,0:T(8,128)(2,1)}) %all-gather.16.cloned.1.call-update) | async-done | bytes 6291472 | tf_op jit(solution)/shard_map/all_gather | solution.py:93
  420.8 3.8 fusion.6
  424.7 90.9 %all-gather.18.cloned.1.call-done = bf16[2048,1536]{1,0:T(8,128)(2,1)} async-done(((bf16[128,1536]{1,0:T(8,128)(2,1)}), bf16[2048,1536]{1,0:T(8,128)(2,1)}) %all-gather.18.cloned.1.call-update) | async-done | bytes 6291472 | tf_op jit(solution)/shard_map/all_gather | solution.py:93
  515.6 3.8 fusion.5
  519.4 112.5 %all-gather.20.cloned.1.call-done = bf16[1536,2048]{1,0:T(8,128)(2,1)} async-done(((bf16[1536,128]{1,0:T(8,128)(2,1)}), bf16[1536,2048]{1,0:T(8,128)(2,1)}) %all-gather.20.cloned.1.call-update) | async-done | bytes 6291472 | tf_op jit(solution)/shard_map/all_gather | solution.py:166
  631.9 5.1 convolution_convert_fusion
  637.0 16.9 %all-reduce.4.cloned.1.call-done = bf16[128,2048]{1,0:T(8,128)(2,1)} async-done(((bf16[128,2048]{1,0:T(8,128)(2,1)}), bf16[128,2048]{1,0:T(8,128)(2,1)}) %all-reduce.4.cloned.1.call-update) | async-done | bytes 524304 | tf_op jit(solution)/shard_map/psum | solution.py:168
  653.9 2.0 fusion.18
  (104 shorter events, 23.5 us)
Async XLA Ops:
  6.5 215.6 %copy-start.1 = (bf16[1024,128]{1,0:T(8,128)(2,1)S(1)}, bf16[1024,128]{1,0:T(8,128)(2,1)}, u32[]{:S(2)}) copy-start(bf16[1024,128]{1,0:T(8,128)(2,1)} %param.21) | copy-start | bytes 786436
  6.5 230.5 %all-gather.10.cloned.1.call-start = ((), (), s32[]{:S(2)}) async-start(), calls=%async_computation.2 | async-start | bytes 2228224 | tf_op jit(solution)/shard_map/all_gather | solution.py:93
  7.3 231.9 %all-gather.8.cloned.1.call-start = ((), (), s32[]{:S(2)}) async-start(), calls=%async_computation.1 | async-start | bytes 2228224 | tf_op jit(solution)/shard_map/all_gather | solution.py:93
  8.0 236.3 %all-gather.12.cloned.1.call-start = ((), (), s32[]{:S(2)}) async-start(), calls=%async_computation.3 | async-start | bytes 4456448 | tf_op jit(solution)/shard_map/all_gather | solution.py:93
  8.7 302.5 %all-gather.14.cloned.1.call-start = ((), (), s32[]{:S(2)}) async-start(), calls=%async_computation.4 | async-start | bytes 4456448 | tf_op jit(solution)/shard_map/all_gather | solution.py:93
  8.8 13.5 %collective-permute-start = (bf16[1024,128]{1,0:T(8,128)(2,1)}, bf16[1024,128]{1,0:T(8,128)(2,1)S(1)}, u32[]{:S(2)}, u32[]{:S(2)}) collective-permute-start(bf16[1024,128]{1,0:T(8,128)(2,1)} %param.21), channel_id=1, source_target_pairs={{0,2},{2,4},{4,6},{6,8},{8,10},{10,12},{12,14},{14,16},{16,18},{18... | collective-permute-start | bytes 786440 | tf_op jit(solution)/shard_map/ppermute | solution.py:145
  22.3 13.8 %collective-permute-start.1 = (bf16[1024,128]{1,0:T(8,128)(2,1)S(1)}, bf16[1024,128]{1,0:T(8,128)(2,1)S(1)}, u32[]{:S(2)}, u32[]{:S(2)}) collective-permute-start(bf16[1024,128]{1,0:T(8,128)(2,1)S(1)} %collective-permute-done), channel_id=1, source_target_pairs={{0,2},{2,4},{4,6},{6,8},{8,10},{10,12},{12,14},{14,16},{16,18},{18... | collective-permute-start | bytes 786440 | tf_op jit(solution)/shard_map/ppermute | solution.py:145
  36.1 14.3 %collective-permute-start.2 = (bf16[1024,128]{1,0:T(8,128)(2,1)S(1)}, bf16[1024,128]{1,0:T(8,128)(2,1)S(1)}, u32[]{:S(2)}, u32[]{:S(2)}) collective-permute-start(bf16[1024,128]{1,0:T(8,128)(2,1)S(1)} %collective-permute-done.1), channel_id=1, source_target_pairs={{0,2},{2,4},{4,6},{6,8},{8,10},{10,12},{12,14},{14,16},{16,18},{18... | collective-permute-start | bytes 786440 | tf_op jit(solution)/shard_map/ppermute | solution.py:145
  50.4 10.0 %collective-permute-start.3 = (bf16[1024,128]{1,0:T(8,128)(2,1)S(1)}, bf16[1024,128]{1,0:T(8,128)(2,1)S(1)}, u32[]{:S(2)}, u32[]{:S(2)}) collective-permute-start(bf16[1024,128]{1,0:T(8,128)(2,1)S(1)} %collective-permute-done.2), channel_id=1, source_target_pairs={{0,2},{2,4},{4,6},{6,8},{8,10},{10,12},{12,14},{14,16},{16,18},{18... | collective-permute-start | bytes 786440 | tf_op jit(solution)/shard_map/ppermute | solution.py:145
  60.4 16.8 %collective-permute-start.4 = (bf16[1024,128]{1,0:T(8,128)(2,1)S(1)}, bf16[1024,128]{1,0:T(8,128)(2,1)S(1)}, u32[]{:S(2)}, u32[]{:S(2)}) collective-permute-start(bf16[1024,128]{1,0:T(8,128)(2,1)S(1)} %collective-permute-done.3), channel_id=1, source_target_pairs={{0,2},{2,4},{4,6},{6,8},{8,10},{10,12},{12,14},{14,16},{16,18},{18... | collective-permute-start | bytes 786440 | tf_op jit(solution)/shard_map/ppermute | solution.py:145
  77.2 11.5 %collective-permute-start.5 = (bf16[1024,128]{1,0:T(8,128)(2,1)S(1)}, bf16[1024,128]{1,0:T(8,128)(2,1)S(1)}, u32[]{:S(2)}, u32[]{:S(2)}) collective-permute-start(bf16[1024,128]{1,0:T(8,128)(2,1)S(1)} %collective-permute-done.4), channel_id=1, source_target_pairs={{0,2},{2,4},{4,6},{6,8},{8,10},{10,12},{12,14},{14,16},{16,18},{18... | collective-permute-start | bytes 786440 | tf_op jit(solution)/shard_map/ppermute | solution.py:145
  88.7 14.5 %collective-permute-start.6 = (bf16[1024,128]{1,0:T(8,128)(2,1)S(1)}, bf16[1024,128]{1,0:T(8,128)(2,1)S(1)}, u32[]{:S(2)}, u32[]{:S(2)}) collective-permute-start(bf16[1024,128]{1,0:T(8,128)(2,1)S(1)} %collective-permute-done.5), channel_id=1, source_target_pairs={{0,2},{2,4},{4,6},{6,8},{8,10},{10,12},{12,14},{14,16},{16,18},{18... | collective-permute-start | bytes 786440 | tf_op jit(solution)/shard_map/ppermute | solution.py:145
  103.2 12.0 %collective-permute-start.7 = (bf16[1024,128]{1,0:T(8,128)(2,1)S(1)}, bf16[1024,128]{1,0:T(8,128)(2,1)S(1)}, u32[]{:S(2)}, u32[]{:S(2)}) collective-permute-start(bf16[1024,128]{1,0:T(8,128)(2,1)S(1)} %collective-permute-done.6), channel_id=1, source_target_pairs={{0,2},{2,4},{4,6},{6,8},{8,10},{10,12},{12,14},{14,16},{16,18},{18... | collective-permute-start | bytes 786440 | tf_op jit(solution)/shard_map/ppermute | solution.py:145
  115.2 13.7 %collective-permute-start.8 = (bf16[1024,128]{1,0:T(8,128)(2,1)S(1)}, bf16[1024,128]{1,0:T(8,128)(2,1)S(1)}, u32[]{:S(2)}, u32[]{:S(2)}) collective-permute-start(bf16[1024,128]{1,0:T(8,128)(2,1)S(1)} %collective-permute-done.7), channel_id=1, source_target_pairs={{0,2},{2,4},{4,6},{6,8},{8,10},{10,12},{12,14},{14,16},{16,18},{18... | collective-permute-start | bytes 786440 | tf_op jit(solution)/shard_map/ppermute | solution.py:145
  129.0 15.8 %collective-permute-start.9 = (bf16[1024,128]{1,0:T(8,128)(2,1)S(1)}, bf16[1024,128]{1,0:T(8,128)(2,1)S(1)}, u32[]{:S(2)}, u32[]{:S(2)}) collective-permute-start(bf16[1024,128]{1,0:T(8,128)(2,1)S(1)} %collective-permute-done.8), channel_id=1, source_target_pairs={{0,2},{2,4},{4,6},{6,8},{8,10},{10,12},{12,14},{14,16},{16,18},{18... | collective-permute-start | bytes 786440 | tf_op jit(solution)/shard_map/ppermute | solution.py:145
  129.0 194.6 %reduce-scatter.2.cloned.1.call-start = ((), (), s32[]{:S(2)}) async-start(), calls=%async_computation.5 | async-start | bytes 786432 | tf_op jit(solution)/shard_map/reduce_scatter | solution.py:149
  144.7 11.2 %collective-permute-start.10 = (bf16[1024,128]{1,0:T(8,128)(2,1)S(1)}, bf16[1024,128]{1,0:T(8,128)(2,1)S(1)}, u32[]{:S(2)}, u32[]{:S(2)}) collective-permute-start(bf16[1024,128]{1,0:T(8,128)(2,1)S(1)} %collective-permute-done.9), channel_id=1, source_target_pairs={{0,2},{2,4},{4,6},{6,8},{8,10},{10,12},{12,14},{14,16},{16,18},{18... | collective-permute-start | bytes 786440 | tf_op jit(solution)/shard_map/ppermute | solution.py:145
  155.9 39.7 %copy-start.2 = (bf16[1024,128]{1,0:T(8,128)(2,1)}, bf16[1024,128]{1,0:T(8,128)(2,1)S(1)}, u32[]{:S(2)}) copy-start(bf16[1024,128]{1,0:T(8,128)(2,1)S(1)} %collective-permute-done.10) | copy-start | bytes 786436
  155.9 10.0 %collective-permute-start.11 = (bf16[1024,128]{1,0:T(8,128)(2,1)S(1)}, bf16[1024,128]{1,0:T(8,128)(2,1)S(1)}, u32[]{:S(2)}, u32[]{:S(2)}) collective-permute-start(bf16[1024,128]{1,0:T(8,128)(2,1)S(1)} %collective-permute-done.10), channel_id=1, source_target_pairs={{0,2},{2,4},{4,6},{6,8},{8,10},{10,12},{12,14},{14,16},{16,18},{18... | collective-permute-start | bytes 786440 | tf_op jit(solution)/shard_map/ppermute | solution.py:145
  165.9 29.8 %copy-start.4 = (bf16[1024,128]{1,0:T(8,128)(2,1)}, bf16[1024,128]{1,0:T(8,128)(2,1)S(1)}, u32[]{:S(2)}) copy-start(bf16[1024,128]{1,0:T(8,128)(2,1)S(1)} %collective-permute-done.11) | copy-start | bytes 786436
  165.9 14.8 %collective-permute-start.12 = (bf16[1024,128]{1,0:T(8,128)(2,1)S(1)}, bf16[1024,128]{1,0:T(8,128)(2,1)S(1)}, u32[]{:S(2)}, u32[]{:S(2)}) collective-permute-start(bf16[1024,128]{1,0:T(8,128)(2,1)S(1)} %collective-permute-done.11), channel_id=1, source_target_pairs={{0,2},{2,4},{4,6},{6,8},{8,10},{10,12},{12,14},{14,16},{16,18},{18... | collective-permute-start | bytes 786440 | tf_op jit(solution)/shard_map/ppermute | solution.py:145
  165.9 29.7 %copy-start.12 = (f32[4]{0:T(128)}, f32[4]{0:T(128)S(1)}, u32[]{:S(2)}) copy-start(f32[4]{0:T(128)S(1)} %subtract_log_fusion) | copy-start | bytes 52
  180.7 0.7 copy-start.6
  181.4 14.2 %collective-permute-start.13 = (bf16[1024,128]{1,0:T(8,128)(2,1)S(1)}, bf16[1024,128]{1,0:T(8,128)(2,1)}, u32[]{:S(2)}, u32[]{:S(2)}) collective-permute-start(bf16[1024,128]{1,0:T(8,128)(2,1)S(1)} %collective-permute-done.12), channel_id=1, source_target_pairs={{0,2},{2,4},{4,6},{6,8},{8,10},{10,12},{12,14},{14,16},{16,18},{18... | collective-permute-start | bytes 786440 | tf_op jit(solution)/shard_map/ppermute | solution.py:145
  195.6 10.3 %collective-permute-start.14 = (bf16[1024,128]{1,0:T(8,128)(2,1)}, bf16[1024,128]{1,0:T(8,128)(2,1)}, u32[]{:S(2)}, u32[]{:S(2)}) collective-permute-start(bf16[1024,128]{1,0:T(8,128)(2,1)} %collective-permute-done.13), channel_id=1, source_target_pairs={{0,2},{2,4},{4,6},{6,8},{8,10},{10,12},{12,14},{14,16},{16,18},{18... | collective-permute-start | bytes 786440 | tf_op jit(solution)/shard_map/ppermute | solution.py:145
  195.6 30.7 %copy-start.7 = (bf16[1024,128]{1,0:T(8,128)(2,1)S(1)}, bf16[1024,128]{1,0:T(8,128)(2,1)}, u32[]{:S(2)}) copy-start(bf16[1024,128]{1,0:T(8,128)(2,1)} %copy-done.6) | copy-start | bytes 786436
  196.5 30.5 %copy-start.5 = (bf16[1024,128]{1,0:T(8,128)(2,1)S(1)}, bf16[1024,128]{1,0:T(8,128)(2,1)}, u32[]{:S(2)}) copy-start(bf16[1024,128]{1,0:T(8,128)(2,1)} %copy-done.4) | copy-start | bytes 786436
  196.5 31.3 %copy-start.3 = (bf16[1024,128]{1,0:T(8,128)(2,1)S(1)}, bf16[1024,128]{1,0:T(8,128)(2,1)}, u32[]{:S(2)}) copy-start(bf16[1024,128]{1,0:T(8,128)(2,1)} %copy-done.2) | copy-start | bytes 786436
  196.5 40.5 %copy-start = (bf16[128,2048]{1,0:T(8,128)(2,1)S(1)}, bf16[128,2048]{1,0:T(8,128)(2,1)}, u32[]{:S(2)}) copy-start(bf16[128,2048]{1,0:T(8,128)(2,1)} %param.14) | copy-start | bytes 1572868
  196.5 40.5 %copy-start.8 = (f32[2048]{0:T(1024)S(1)}, f32[2048]{0:T(1024)}, u32[]{:S(2)}) copy-start(f32[2048]{0:T(1024)} %param.15) | copy-start | bytes 24580
  229.4 14.8 %copy-start.13 = (f32[128]{0:T(128)S(1)}, f32[128]{0:T(128)}, u32[]{:S(2)}) copy-start(f32[128]{0:T(128)} %add_rsqrt_fusion.1) | copy-start | bytes 1540
  241.2 70.0 %copy-start.14 = (f32[1024]{0:T(1024)S(1)}, f32[1024]{0:T(1024)}, u32[]{:S(2)}) copy-start(f32[1024]{0:T(1024)} %param.20) | copy-start | bytes 12292
  247.8 71.3 %copy-start.10 = (f32[3,1536]{1,0:T(4,128)S(1)}, f32[3,1536]{1,0:T(4,128)}, u32[]{:S(2)}) copy-start(f32[3,1536]{1,0:T(4,128)} %param.26) | copy-start | bytes 55300
  247.8 71.3 %copy-start.11 = (f32[3,1536]{1,0:T(4,128)S(1)}, f32[3,1536]{1,0:T(4,128)}, u32[]{:S(2)}) copy-start(f32[3,1536]{1,0:T(4,128)} %param.25) | copy-start | bytes 55300
  248.0 172.8 %copy-start.9 = (f32[2048]{0:T(1024)S(1)}, f32[2048]{0:T(1024)}, u32[]{:S(2)}) copy-start(f32[2048]{0:T(1024)} %param.22) | copy-start | bytes 24580
  317.0 103.9 %all-gather.16.cloned.1.call-start = ((), (), s32[]{:S(2)}) async-start(), calls=%async_computation.6 | async-start | bytes 6684672 | tf_op jit(solution)/shard_map/all_gather | solution.py:93
  317.6 198.0 %all-gather.18.cloned.1.call-start = ((), (), s32[]{:S(2)}) async-start(), calls=%async_computation.7 | async-start | bytes 6684672 | tf_op jit(solution)/shard_map/all_gather | solution.py:93
  318.3 313.6 %all-gather.20.cloned.1.call-start = ((), (), s32[]{:S(2)}) async-start(), calls=%async_computation.8 | async-start | bytes 6684672 | tf_op jit(solution)/shard_map/all_gather | solution.py:166
  319.1 334.8 %all-reduce.4.cloned.1.call-start = ((), (), s32[]{:S(2)}) async-start(), calls=%async_computation.9 | async-start | bytes 1048576 | tf_op jit(solution)/shard_map/psum | solution.py:168
Sparse Core Ops, SparseCore 0:
  10.1 71.8 all-gather.9
  84.8 68.7 all-gather.7
  156.4 78.0 all-gather.11
  237.0 74.1 all-gather.13
  317.1 6.5 reduce-scatter.1
  326.3 94.4 all-gather.15
  423.6 91.9 all-gather.17
  518.3 113.5 all-gather.19
  637.1 16.7 all-reduce.3
